TPU v7x, 32 devices: a whole 2x2x4 slice. The times are simulated.
32 devices in a mesh: sp: 8 (over z, x), dp: 4 (over y, core).
Axes of the slice: x: 2, y: 2, z: 4, core: 2. Of those that a mesh axis runs over, the one named last changes fastest.
Arguments:
- queries: bfloat16 [4, 1024, 2048], P('dp', 'sp'), may hold values from -9 to 9
- keys: bfloat16 [4, 1024, 512], P('dp', 'sp'), may hold values from -9 to 9
- values: bfloat16 [4, 1024, 512], P('dp', 'sp'), may hold values from -6 to 6
- out_grad: bfloat16 [4, 1024, 2048], P('dp', 'sp'), may hold values from -24 to 24
- layer_in: bfloat16 [4, 1024, 4096], P('dp', 'sp'), may hold values from -0.1875 to 0.1875
- key_weight: bfloat16 [4096, 512], P('dp'), may hold values from -0.09375 to 0.09375
- value_weight: bfloat16 [4096, 512], P('dp'), may hold values from -0.09375 to 0.09375
- query_gain: float32 [128], replicated, may hold values from 0.64 to 6.04
- key_gain: float32 [128], replicated, may hold values from 0.64 to 6.04
Outputs:
- grad_query: bfloat16 [4, 1024, 2048], P('dp', 'sp')
- grad_in: bfloat16 [4, 1024, 4096], P('dp', 'sp')
- grad_key_weight: float32 [4096, 512], P('dp')
- grad_value_weight: float32 [4096, 512], P('dp')
All inputs are finite; a program needn't handle non-finite values.
Results may differ from a plain program's by a relative error of at most 0.018.
The roundings to bfloat16 on the way count: a program that leaves them out, or rounds other values in their place, can miss the bound.
Values may be sent and summed in bfloat16 or wider, within the bound.
A program may use at most 128 MiB of HBM per device.

v0:
```python
from functools import partial
import math
import jax
import jax.numpy as jnp
from jax import lax
from jax.sharding import PartitionSpec as P

HEADS = 16
KV_HEADS = 4
HEAD_DIM = 128
GRID_W = 64
epsilon = 1e-06
rope_base = 10000.0


def norm_rotate(vector, gain_vec, row_index, col_index):
    scaled = (
        vector * lax.rsqrt(jnp.mean(vector * vector, axis=-1, keepdims=True) + epsilon) * gain_vec
    )
    quarter = vector.shape[-1] // 4
    inverse = rope_base ** (-jnp.arange(quarter, dtype=jnp.float32) / quarter)
    pieces = []
    for offset, position in ((0, row_index), (2 * quarter, col_index)):
        angles = position.astype(jnp.float32)[:, None] * inverse[None, :]
        cosine = jnp.cos(angles)
        sine_part = jnp.sin(angles)
        first_half = scaled[:, offset : offset + quarter]
        second_half = scaled[:, offset + quarter : offset + 2 * quarter]
        pieces.append(first_half * cosine - second_half * sine_part)
        pieces.append(first_half * sine_part + second_half * cosine)
    return jnp.concatenate(pieces, axis=1)


def contract_cols(left_side, right_side):
    return lax.dot_general(
        left_side, right_side, (((1,), (1,)), ((), ())), preferred_element_type=jnp.float32
    )


def contract_rows(left_side, right_side):
    return lax.dot_general(
        left_side, right_side, (((0,), (0,)), ((), ())), preferred_element_type=jnp.float32
    )


def head_grads(query_rows, grad_rows, key_rows, value_rows, query_gain, key_gain):
    length = query_rows.shape[0]
    block_rows = math.gcd(length, 512)
    positions = jnp.arange(length, dtype=jnp.int32)
    row_index = positions // GRID_W
    col_index = positions % GRID_W
    q_rot, q_back = jax.vjp(
        partial(norm_rotate, gain_vec=query_gain, row_index=row_index, col_index=col_index),
        query_rows.astype(jnp.float32),
    )
    k_rot, k_back = jax.vjp(
        partial(norm_rotate, gain_vec=key_gain, row_index=row_index, col_index=col_index),
        key_rows.astype(jnp.float32),
    )
    q_bf = q_rot.astype(jnp.bfloat16)
    k_bf = k_rot.astype(jnp.bfloat16)
    score_scale = q_rot.shape[-1] ** (-0.5)

    def one_block(accums, block_index):
        k_acc, v_acc = accums
        row_start = block_index * block_rows
        q_block = lax.dynamic_slice_in_dim(q_bf, row_start, block_rows, 0)
        g_block = lax.dynamic_slice_in_dim(grad_rows, row_start, block_rows, 0)
        scores = contract_cols(q_block, k_bf) * score_scale
        shifted = jnp.exp(scores - jnp.max(scores, axis=1, keepdims=True))
        attn_probs = shifted / jnp.sum(shifted, axis=1, keepdims=True)
        probs_b = attn_probs.astype(jnp.bfloat16)
        attn_out = jnp.dot(probs_b, value_rows, preferred_element_type=jnp.float32)
        row_delta = jnp.sum(g_block.astype(jnp.float32) * attn_out, axis=1, keepdims=True)
        grad_probs = contract_cols(g_block, value_rows)
        grad_scores = (attn_probs * (grad_probs - row_delta)).astype(jnp.bfloat16)
        q_grad = jnp.dot(grad_scores, k_bf, preferred_element_type=jnp.float32) * score_scale
        k_acc = k_acc + contract_rows(grad_scores, q_block) * score_scale
        v_acc = v_acc + contract_rows(probs_b, g_block)
        return ((k_acc, v_acc), q_grad)

    zeros_init = jnp.zeros(query_rows.shape, jnp.float32)
    (k_acc, v_acc), q_grads = lax.scan(
        one_block, (zeros_init, zeros_init), jnp.arange(length // block_rows, dtype=jnp.int32)
    )
    grad_rq = q_grads.reshape(length, query_rows.shape[1])
    grad_q = q_back(grad_rq)[0].astype(jnp.bfloat16)
    grad_k = k_back(k_acc)[0].astype(jnp.bfloat16)
    return (grad_q, grad_k, v_acc.astype(jnp.bfloat16))


def on_device(
    queries, keys, values, out_grad, layer_in, key_weight, value_weight, query_gain, key_gain
):
    seq_count, tokens_here, _ = queries.shape
    model_width = layer_in.shape[2]
    group_size = HEADS // KV_HEADS
    kv_width = KV_HEADS * HEAD_DIM
    query_part = queries.reshape(seq_count, tokens_here, HEADS, HEAD_DIM)
    grad_part = out_grad.reshape(seq_count, tokens_here, HEADS, HEAD_DIM)
    shape_wide = (seq_count, tokens_here, KV_HEADS, group_size, HEAD_DIM)
    key_part = jnp.broadcast_to(
        keys.reshape(seq_count, tokens_here, KV_HEADS, 1, HEAD_DIM), shape_wide
    ).reshape(seq_count, tokens_here, HEADS, HEAD_DIM)
    value_part = jnp.broadcast_to(
        values.reshape(seq_count, tokens_here, KV_HEADS, 1, HEAD_DIM), shape_wide
    ).reshape(seq_count, tokens_here, HEADS, HEAD_DIM)
    bundle = jnp.concatenate([query_part, grad_part, key_part, value_part], axis=3)
    arrived = lax.all_to_all(bundle, "sp", split_axis=2, concat_axis=1, tiled=True)
    arrived_seqs, length, head_count, _ = arrived.shape
    flat_heads = arrived.transpose(0, 2, 1, 3).reshape(
        arrived_seqs * head_count, length, 4 * HEAD_DIM
    )

    def one_item(one_head):
        grad_q, grad_k, grad_v = head_grads(
            one_head[:, :HEAD_DIM],
            one_head[:, HEAD_DIM : 2 * HEAD_DIM],
            one_head[:, 2 * HEAD_DIM : 3 * HEAD_DIM],
            one_head[:, 3 * HEAD_DIM :],
            query_gain,
            key_gain,
        )
        return jnp.concatenate([grad_q, grad_k, grad_v], axis=1)

    all_grads = lax.map(one_item, flat_heads)
    head_out = all_grads.reshape(arrived_seqs, head_count, length, 3 * HEAD_DIM).transpose(
        0, 2, 1, 3
    )
    token_grads = lax.all_to_all(head_out, "sp", split_axis=1, concat_axis=2, tiled=True)
    grad_query = token_grads[:, :, :, :HEAD_DIM].reshape(seq_count, tokens_here, HEADS * HEAD_DIM)

    def grouped(array):
        summed = jnp.sum(
            array.reshape(seq_count * tokens_here, KV_HEADS, group_size, HEAD_DIM).astype(
                jnp.float32
            ),
            axis=2,
        )
        return summed.astype(jnp.bfloat16).reshape(seq_count * tokens_here, kv_width)

    kv_grad = jnp.concatenate(
        [
            grouped(token_grads[:, :, :, HEAD_DIM : 2 * HEAD_DIM]),
            grouped(token_grads[:, :, :, 2 * HEAD_DIM :]),
        ],
        axis=1,
    )
    stacked = jnp.concatenate([key_weight, value_weight], axis=1)
    grad_flat = contract_cols(kv_grad, lax.all_gather(stacked, "dp", axis=0, tiled=True))
    grad_in = grad_flat.astype(jnp.bfloat16).reshape(seq_count, tokens_here, model_width)
    flat_in = layer_in.reshape(seq_count * tokens_here, model_width)
    partial_sum = lax.psum_scatter(
        contract_rows(flat_in, kv_grad).astype(jnp.bfloat16), "dp", scatter_dimension=0, tiled=True
    )
    weight_grad = lax.psum(partial_sum, "sp").astype(jnp.float32)
    return (grad_query, grad_in, weight_grad[:, :kv_width], weight_grad[:, kv_width:])


def solution(mesh):
    in_specs = (
        P("dp", "sp", None),
        P("dp", "sp", None),
        P("dp", "sp", None),
        P("dp", "sp", None),
        P("dp", "sp", None),
        P("dp", None),
        P("dp", None),
        P(),
        P(),
    )
    out_specs = (P("dp", "sp", None), P("dp", "sp", None), P("dp", None), P("dp", None))
    return jax.shard_map(
        on_device, mesh=mesh, in_specs=in_specs, out_specs=out_specs, check_vma=False
    )
```

profile of v0, /device:TPU:0, one launch (start us, length us, event | category | flops | bytes accessed | tf_op | source)
XLA Modules:
  0.0 448.0 jit_solution(12907583575697410862)
XLA Ops:
  10.6 1.3 copy.112
  12.2 1.5 maximum_bitcast_fusion.1
  13.7 7.3 %all-to-all-start = ((bf16[1,128,16,512]{1,3,0,2:T(8,128)(2,1)}), bf16[1,128,16,512]{1,3,0,2:T(8,128)(2,1)S(1)}, u32[]{:S(2)}, u32[]{:S(2)}) async-start(bf16[1,128,16,512]{1,3,0,2:T(8,128)(2,1)} %maximum_bitcast_fusion.1), calls=%async_computation | async-start | bytes 4194304 | tf_op jit(solution)/shard_map/all_to_all | solution.py:109
  21.0 48.2 %all-to-all-done = bf16[1,128,16,512]{1,3,0,2:T(8,128)(2,1)S(1)} async-done(((bf16[1,128,16,512]{1,3,0,2:T(8,128)(2,1)}), bf16[1,128,16,512]{1,3,0,2:T(8,128)(2,1)S(1)}, u32[]{:S(2)}, u32[]{:S(2)}) %all-to-all-start) | async-done | bytes 2097184 | tf_op jit(solution)/shard_map/all_to_all | solution.py:109
  69.2 2.6 copy.116
  71.8 3.1 copy.117
  74.9 69.9 %while.43 = (s32[]{:T(128)}, bf16[2,1024,384]{1,2,0:T(8,128)(2,1)}, bf16[2,1024,512]{2,1,0:T(8,128)(2,1)}, f32[128]{0:T(128)}, f32[128]{0:T(128)}, /*index=5*/s3...) while((s32[]{:T(128)}, bf16[2,1024,384]{1,2,0:T(8,128)(2,1)}, ...), condition=%wide.region_10.11_spmd, body=%wide.region_0.10_spmd.sunk | while | flops 825649728 | bytes 72149696 | solution.py:126
  74.9 2.3 constant_dynamic-slice_fusion.2
  77.2 1.5 copy.146
  84.2 12.8 %while.44 = (s32[]{:T(128)}, f32[1024,128]{1,0:T(8,128)S(1)}, f32[1024,128]{1,0:T(8,128)S(1)}, f32[2,512,128]{2,1,0:T(8,128)}, s32[2]{0:T(128)S(1)}, /*index=5*/...) while((s32[]{:T(128)}, f32[1024,128]{1,0:T(8,128)S(1)}, ...), condition=%wide.region_7.7_spmd.clone, body=%wide.region_3.6_spmd.clone.sunk | while | flops 813038080 | bytes 26097944 | solution.py:83
  98.0 1.6 fusion.145
  99.7 2.0 copy.151
  101.7 1.9 copy.153
  104.4 2.1 fusion.146
  109.9 2.3 constant_dynamic-slice_fusion.2
  112.2 1.5 copy.146
  119.1 12.8 %while.44 = (s32[]{:T(128)}, f32[1024,128]{1,0:T(8,128)S(1)}, f32[1024,128]{1,0:T(8,128)S(1)}, f32[2,512,128]{2,1,0:T(8,128)}, s32[2]{0:T(128)S(1)}, /*index=5*/...) while((s32[]{:T(128)}, f32[1024,128]{1,0:T(8,128)S(1)}, ...), condition=%wide.region_7.7_spmd.clone, body=%wide.region_3.6_spmd.clone.sunk | while | flops 813038080 | bytes 26097944 | solution.py:83
  132.9 1.6 fusion.145
  134.7 2.0 copy.151
  136.7 1.9 copy.153
  139.4 2.1 fusion.146
  144.8 4.3 copy.119
  149.1 40.6 %all_to_all.36 = bf16[1,1024,2,384]{3,2,0,1:T(2,128)(2,1)S(1)} all-to-all(bf16[1,1024,2,384]{3,2,0,1:T(2,128)(2,1)S(1)} %bitcast.84), channel_id=1, replica_groups=mesh['sp'=8,'dp'=4] {'sp'}, dimensions={1} | all-to-all | bytes 3145728 | tf_op jit(solution)/shard_map/all_to_all | solution.py:130
  191.0 5.5 %convert_bitcast_fusion = bf16[4096,1024]{0,1:T(8,128)(2,1)} fusion(bf16[1,128,4096]{2,1,0:T(8,128)(2,1)S(1)} %copy-done, bf16[128,512]{0,1:T(8,128)(2,1)S(1)} %bitcast.95, bf16[128,512]{0,1:T(8,128)(2,1)S(1)} %bitcast.93), kind=kOutput, calls=%fused_computation.129 | convolution fusion | flops 1078460416 | bytes 9699328 | tf_op jit(solution)/shard_map/dot_general | solution.py:41
  197.8 2.9 pad_maximum_fusion.2
  200.7 66.4 %reduce-scatter.2.cloned.1.call-done = bf16[1024,1024]{0,1:T(8,128)(2,1)} async-done(((bf16[4096,1024]{0,1:T(8,128)(2,1)}), bf16[1024,1024]{0,1:T(8,128)(2,1)}) %reduce-scatter.2.cloned.1.call-update) | async-done | bytes 2097168 | tf_op jit(solution)/shard_map/reduce_scatter | solution.py:153
  268.4 59.1 %all-gather.2.cloned.1.call-done = bf16[4096,1024]{1,0:T(8,128)(2,1)} async-done(((bf16[1024,1024]{1,0:T(8,128)(2,1)}), bf16[4096,1024]{1,0:T(8,128)(2,1)}) %all-gather.2.cloned.1.call-update) | async-done | bytes 8388624 | tf_op jit(solution)/shard_map/all_gather | solution.py:150
  327.5 7.2 %fusion.93 = bf16[1,128,4096]{2,1,0:T(8,128)(2,1)} fusion(bf16[4096,1024]{1,0:T(8,128)(2,1)} %all-gather.2.cloned.1.call-done, bf16[128,512]{0,1:T(8,128)(2,1)S(1)} %bitcast.96, bf16[128,512]{0,1:T(8,128)(2,1)S(1)} %bitcast.94), kind=kOutput, calls=%fused_computation.131 | convolution fusion | flops 1074790400 | bytes 9699328 | tf_op jit(solution)/shard_map/dot_general | solution.py:35
  334.8 98.7 %all-reduce.10.cloned.1.call-done = bf16[1024,1024]{0,1:T(8,128)(2,1)} async-done(((bf16[1024,1024]{0,1:T(8,128)(2,1)}), bf16[1024,1024]{0,1:T(8,128)(2,1)}) %all-reduce.10.cloned.1.call-update) | async-done | bytes 2097168 | tf_op jit(solution)/shard_map/psum | solution.py:156
  433.5 3.3 fusion.99
  436.8 2.9 copy.127
  439.7 1.8 copy.126
  (171 shorter events, 51.4 us)
Async XLA Ops:
  7.2 183.9 %copy-start = (bf16[1,128,4096]{2,1,0:T(8,128)(2,1)S(1)}, bf16[1,128,4096]{2,1,0:T(8,128)(2,1)}, u32[]{:S(2)}) copy-start(bf16[1,128,4096]{2,1,0:T(8,128)(2,1)} %param.17) | copy-start | bytes 3145732
  13.7 55.5 %all-to-all-start = ((bf16[1,128,16,512]{1,3,0,2:T(8,128)(2,1)}), bf16[1,128,16,512]{1,3,0,2:T(8,128)(2,1)S(1)}, u32[]{:S(2)}, u32[]{:S(2)}) async-start(bf16[1,128,16,512]{1,3,0,2:T(8,128)(2,1)} %maximum_bitcast_fusion.1), calls=%async_computation | async-start | bytes 4194304 | tf_op jit(solution)/shard_map/all_to_all | solution.py:109
  21.0 246.2 %reduce-scatter.2.cloned.1.call-start = ((), (), s32[]{:S(2)}) async-start(), calls=%async_computation.4 | async-start | bytes 10485760 | tf_op jit(solution)/shard_map/reduce_scatter | solution.py:153
  74.9 7.8 %copy-start.14 = (f32[32]{0:T(128)}, f32[32]{0:T(128)S(1)}, u32[]{:S(2)}) copy-start(f32[32]{0:T(128)S(1)} %multiply_power_fusion.2) | copy-start | bytes 388 | tf_op jit(solution)/shard_map/while
  78.7 1.6 copy-start.1
  78.8 5.1 %copy-start.12 = (f32[1024]{0:T(1024)}, f32[1024]{0:T(1024)S(1)}, u32[]{:S(2)}) copy-start(f32[1024]{0:T(1024)S(1)} %get-tuple-element.490) | copy-start | bytes 12292 | tf_op jit(solution)/shard_map/while
  88.1 1.1 copy-start.3
  94.5 1.2 copy-start.3
  96.1 0.8 copy-start.4
  96.9 1.0 copy-start.5
  99.6 4.0 copy-start.6
  99.7 6.8 %copy-start.2 = (bf16[1,1024,512]{1,2,0:T(8,128)(2,1)S(1)}, bf16[1,1024,512]{1,2,0:T(8,128)(2,1)}, u32[]{:S(2)}) copy-start(bf16[1,1024,512]{1,2,0:T(8,128)(2,1)} %copy-done.1) | copy-start | bytes 3145732 | tf_op jit(solution)/shard_map/while
  104.4 3.2 copy-start.11
  104.4 3.2 copy-start.13
  106.6 2.0 copy-start.7
  108.7 1.1 copy-start.8
  109.8 7.8 %copy-start.14 = (f32[32]{0:T(128)}, f32[32]{0:T(128)S(1)}, u32[]{:S(2)}) copy-start(f32[32]{0:T(128)S(1)} %multiply_power_fusion.2) | copy-start | bytes 388 | tf_op jit(solution)/shard_map/while
  113.7 1.6 copy-start.1
  113.8 5.1 %copy-start.12 = (f32[1024]{0:T(1024)}, f32[1024]{0:T(1024)S(1)}, u32[]{:S(2)}) copy-start(f32[1024]{0:T(1024)S(1)} %get-tuple-element.490) | copy-start | bytes 12292 | tf_op jit(solution)/shard_map/while
  123.1 1.2 copy-start.3
  124.7 0.8 copy-start.4
  129.5 1.2 copy-start.3
  131.9 1.0 copy-start.5
  134.5 4.0 copy-start.6
  134.7 6.8 %copy-start.2 = (bf16[1,1024,512]{1,2,0:T(8,128)(2,1)S(1)}, bf16[1,1024,512]{1,2,0:T(8,128)(2,1)}, u32[]{:S(2)}) copy-start(bf16[1,1024,512]{1,2,0:T(8,128)(2,1)} %copy-done.1) | copy-start | bytes 3145732 | tf_op jit(solution)/shard_map/while
  139.4 3.2 copy-start.11
  139.4 3.2 copy-start.13
  141.5 2.0 copy-start.7
  143.6 1.1 copy-start.8
  196.6 1.2 copy-start.9
  196.6 130.9 %all-gather.2.cloned.1.call-start = ((), (), s32[]{:S(2)}) async-start(), calls=%async_computation.3 | async-start | bytes 10485760 | tf_op jit(solution)/shard_map/all_gather | solution.py:150
  200.7 232.8 %all-reduce.10.cloned.1.call-start = ((), (), s32[]{:S(2)}) async-start(), calls=%async_computation.5 | async-start | bytes 4194304 | tf_op jit(solution)/shard_map/psum | solution.py:156
  (4 other events, 3.1 us)
Sparse Core Ops, SparseCore 0:
  196.7 70.3 reduce-scatter.1
  269.3 58.2 all-gather.1
  331.2 102.2 all-reduce.9
where the time goes:
time: 449 us; the launch traced here: 448 us
  waiting for transfers between devices  272 us (61%)
  local copies, waits for them, and re-layouts  62.2 us (14%)
  blocking collectives  40.6 us (9%)
  matrix products  26 us (6%)
  other arithmetic  22.1 us (5%)
  between operations  13.9 us (3%)
  starting transfers between devices  7.4 us (2%)
    psum x1, waiting for transfers between devices, on_device(): weight_grad = lax.psum(partial_sum, 'sp').astype(jnp.float32)  98.7 us
    reduce_scatter x1, waiting for transfers between devices, on_device(): lax.psum_scatter(contract_rows(flat_in, kv_grad).astype(jnp.bfloat16), 'd...  66.4 us
    all_gather x1, waiting for transfers between devices, on_device(): lax.all_gather(stacked, 'dp', axis=0, tiled=True)  59.1 us
    all_to_all x1, waiting for transfers between devices, on_device(): lax.all_to_all(bundle, 'sp', split_axis=2, concat_axis=1, tiled=True)  48.2 us
    all_to_all x1, blocking collectives, on_device(): lax.all_to_all(head_out, 'sp', split_axis=1, concat_axis=2, tiled=True)  40.6 us
    while x72, local copies, waits for them, and re-layouts  20.6 us
    dot_general x9, matrix products, contract_cols(): lax.dot_general(left_side, right_side, (((1,), (1,)), ((), ())), preferre...  11.5 us
    dot_general x9, matrix products, contract_rows(): lax.dot_general(left_side, right_side, (((0,), (0,)), ((), ())), preferre...  10.7 us
  transfers between devices with their start and end apart: 4, of which 4 were waited for; matrix products, arithmetic and copies ran while one was open for 3% of the time, Pallas kernels for 0%

commit v1 on v0

--- a/solution.py
+++ b/solution.py
@@ -153,7 +153,7 @@
     partial_sum = lax.psum_scatter(
         contract_rows(flat_in, kv_grad).astype(jnp.bfloat16), "dp", scatter_dimension=0, tiled=True
     )
-    weight_grad = lax.psum(partial_sum, "sp").astype(jnp.float32)
+    weight_grad = jnp.sum(lax.all_gather(partial_sum, "sp"), axis=0).astype(jnp.float32)
     return (grad_query, grad_in, weight_grad[:, :kv_width], weight_grad[:, kv_width:])
 
 

time: 449 us -> 617 us (1.37)
  waiting for transfers between devices: 272 us -> 396 us
  matrix products: 26 us -> 50.4 us
  other arithmetic: 22.1 us -> 34.5 us
  local copies, waits for them, and re-layouts: 62.2 us -> 69.6 us
    all_gather x0 -> x1, waiting for transfers between devices: none -> 222 us  [on_device(): lax.all_gather(partial_sum, 'sp')]
    psum x1 -> x0, waiting for transfers between devices: 98.7 us -> none  [on_device(): weight_grad = lax.psum(partial_sum, 'sp').astype(jnp.float32)]
    unnamed x9 -> x14, local copies, waits for them, and re-layouts: 9.49 us -> 25.1 us
    dot_general x9, matrix products: 10.7 us -> 23.6 us  [contract_rows(): lax.dot_general(left_side, right_side, (((0,), (0,)), ((), ())), preferre...]
    reduce_sum x0 -> x1, other arithmetic: none -> 11.6 us  [on_device(): jnp.sum(lax.all_gather(partial_sum, 'sp'), axis=0).astype(jnp.float32)]
    while x72 -> x92, local copies, waits for them, and re-layouts: 20.6 us -> 12.3 us
    dot_general x9, matrix products: 11.5 us -> 19.4 us  [contract_cols(): lax.dot_general(left_side, right_side, (((1,), (1,)), ((), ())), preferre...]
  transfers between devices with their start and end apart: 4 -> 4, of which waited for: 4 -> 4; matrix products, arithmetic and copies ran while one was open for 3% -> 2% of each run, Pallas kernels for 0% -> 0%
where the time goes in v1:
time: 617 us; the launch traced here: 616 us
  waiting for transfers between devices  396 us (64%)
  local copies, waits for them, and re-layouts  69.6 us (11%)
  matrix products  50.4 us (8%)
  blocking collectives  40.6 us (7%)
  other arithmetic  34.5 us (6%)
  between operations  13.9 us (2%)
  starting transfers between devices  7.4 us (1%)
    all_gather x1, waiting for transfers between devices, on_device(): lax.all_gather(partial_sum, 'sp')  222 us
    reduce_scatter x1, waiting for transfers between devices, on_device(): lax.psum_scatter(contract_rows(flat_in, kv_grad).astype(jnp.bfloat16), 'd...  66.4 us
    all_gather x1, waiting for transfers between devices, on_device(): lax.all_gather(stacked, 'dp', axis=0, tiled=True)  59.1 us
    all_to_all x1, waiting for transfers between devices, on_device(): lax.all_to_all(bundle, 'sp', split_axis=2, concat_axis=1, tiled=True)  48.2 us
    all_to_all x1, blocking collectives, on_device(): lax.all_to_all(head_out, 'sp', split_axis=1, concat_axis=2, tiled=True)  40.6 us
    unnamed x14, local copies, waits for them, and re-layouts  25.1 us
    dot_general x9, matrix products, contract_rows(): lax.dot_general(left_side, right_side, (((0,), (0,)), ((), ())), preferre...  23.6 us
    dot_general x9, matrix products, contract_cols(): lax.dot_general(left_side, right_side, (((1,), (1,)), ((), ())), preferre...  19.4 us
  transfers between devices with their start and end apart: 4, of which 4 were waited for; matrix products, arithmetic and copies ran while one was open for 2% of the time, Pallas kernels for 0%

profile of v1, /device:TPU:0, one launch (start us, length us, event | category | flops | bytes accessed | tf_op | source)
XLA Modules:
  0.0 615.6 jit_solution(16376986813575345866)
XLA Ops:
  13.7 7.3 %all-to-all-start = ((bf16[1,128,16,512]{1,3,0,2:T(8,128)(2,1)}), bf16[1,128,16,512]{1,3,0,2:T(8,128)(2,1)S(1)}, u32[]{:S(2)}, u32[]{:S(2)}) async-start(bf16[1,128,16,512]{1,3,0,2:T(8,128)(2,1)} %maximum_bitcast_fusion.1), calls=%async_computation | async-start | bytes 4194304 | tf_op jit(solution)/shard_map/all_to_all | solution.py:109
  21.0 48.2 %all-to-all-done = bf16[1,128,16,512]{1,3,0,2:T(8,128)(2,1)S(1)} async-done(((bf16[1,128,16,512]{1,3,0,2:T(8,128)(2,1)}), bf16[1,128,16,512]{1,3,0,2:T(8,128)(2,1)S(1)}, u32[]{:S(2)}, u32[]{:S(2)}) %all-to-all-start) | async-done | bytes 2097184 | tf_op jit(solution)/shard_map/all_to_all | solution.py:109
  69.2 2.6 copy.110
  71.8 3.1 copy.111
  74.9 88.3 %while.43 = (s32[]{:T(128)}, bf16[2,1024,384]{1,2,0:T(8,128)(2,1)}, bf16[2,1024,512]{2,1,0:T(8,128)(2,1)}, f32[128]{0:T(128)S(1)}, f32[128]{0:T(128)S(1)}, /*ind...) while((s32[]{:T(128)}, bf16[2,1024,384]{1,2,0:T(8,128)(2,1)}, ...), condition=%wide.region_10.11_spmd, body=%wide.region_0.10_spmd.sunk | while | flops 825649728 | bytes 65338612 | solution.py:126
  81.0 25.9 %while.44 = (s32[]{:T(128)}, f32[1024,128]{1,0:T(8,128)}, f32[1024,128]{1,0:T(8,128)}, f32[2,512,128]{2,1,0:T(8,128)}, s32[2]{0:T(128)S(1)}, /*index=5*/bf16[102...) while((s32[]{:T(128)}, f32[1024,128]{1,0:T(8,128)}, ...), condition=%wide.region_7.7_spmd.clone, body=%wide.region_3.6_spmd.clone.sunk | while | flops 813038080 | bytes 32389476 | solution.py:83
  87.3 2.6 fusion.164
  94.6 1.6 multiply_reduce_fusion.2
  99.6 2.8 fusion.164
  104.6 2.3 convolution_add_fusion.2
  106.9 3.2 fusion.145
  112.8 2.1 fusion.146
  125.1 25.9 %while.44 = (s32[]{:T(128)}, f32[1024,128]{1,0:T(8,128)}, f32[1024,128]{1,0:T(8,128)}, f32[2,512,128]{2,1,0:T(8,128)}, s32[2]{0:T(128)S(1)}, /*index=5*/bf16[102...) while((s32[]{:T(128)}, f32[1024,128]{1,0:T(8,128)}, ...), condition=%wide.region_7.7_spmd.clone, body=%wide.region_3.6_spmd.clone.sunk | while | flops 813038080 | bytes 32389476 | solution.py:83
  131.4 2.6 fusion.164
  138.7 1.6 multiply_reduce_fusion.2
  143.8 2.8 fusion.164
  148.7 2.3 convolution_add_fusion.2
  151.1 3.2 fusion.145
  157.0 2.1 fusion.146
  163.2 4.3 copy.113
  167.5 40.6 %all_to_all.36 = bf16[1,1024,2,384]{3,2,0,1:T(2,128)(2,1)S(1)} all-to-all(bf16[1,1024,2,384]{3,2,0,1:T(2,128)(2,1)S(1)} %bitcast.90), channel_id=1, replica_groups=mesh['sp'=8,'dp'=4] {'sp'}, dimensions={1} | all-to-all | bytes 3145728 | tf_op jit(solution)/shard_map/all_to_all | solution.py:130
  209.4 5.5 convert_bitcast_fusion
  216.2 2.9 pad_maximum_fusion.2
  219.1 66.4 %reduce-scatter.2.cloned.1.call-done = bf16[1024,1024]{0,1:T(8,128)(2,1)} async-done(((bf16[4096,1024]{0,1:T(8,128)(2,1)}), bf16[1024,1024]{0,1:T(8,128)(2,1)}) %reduce-scatter.2.cloned.1.call-update) | async-done | bytes 2097168 | tf_op jit(solution)/shard_map/reduce_scatter | solution.py:153
  286.8 59.1 %all-gather.4.cloned.1.call-done = bf16[4096,1024]{1,0:T(8,128)(2,1)} async-done(((bf16[1024,1024]{1,0:T(8,128)(2,1)}), bf16[4096,1024]{1,0:T(8,128)(2,1)}) %all-gather.4.cloned.1.call-update) | async-done | bytes 8388624 | tf_op jit(solution)/shard_map/all_gather | solution.py:150
  345.9 7.2 %fusion.93 = bf16[1,128,4096]{2,1,0:T(8,128)(2,1)} fusion(bf16[4096,1024]{1,0:T(8,128)(2,1)} %all-gather.4.cloned.1.call-done, bf16[128,512]{0,1:T(8,128)(2,1)S(1)} %bitcast.102, bf16[128,512]{0,1:T(8,128)(2,1)S(1)} %bitcast.100), kind=kOutput, calls=%fused_computation.132 | convolution fusion | flops 1074790400 | bytes 9699328 | tf_op jit(solution)/shard_map/dot_general | solution.py:35
  353.2 222.2 %all-gather.6.cloned.1.call-done = bf16[8192,1024]{0,1:T(8,128)(2,1)} async-done(((bf16[1024,1024]{0,1:T(8,128)(2,1)}), bf16[8192,1024]{0,1:T(8,128)(2,1)}) %all-gather.6.cloned.1.call-update) | async-done | bytes 16777232 | tf_op jit(solution)/shard_map/all_gather | solution.py:156
  575.4 15.6 %copy.131 = bf16[128,8,8,1024]{3,2,1,0:T(8,128)(2,1)S(1)} copy(bf16[128,8,8,1024]{3,1,2,0:T(8,128)(2,1)} %bitcast.87) | data formatting | bytes 33554432
  591.0 11.6 %bitcast_reduce_fusion = bf16[1024,1024]{0,1:T(8,128)(2,1)S(1)} fusion(bf16[128,8,8,1024]{3,2,1,0:T(8,128)(2,1)S(1)} %copy.131), kind=kLoop, calls=%fused_computation.129 | loop fusion | flops 7340032 | bytes 18874368 | tf_op jit(solution)/shard_map/reduce_sum | solution.py:156
  602.6 1.8 fusion.99
  604.4 2.9 copy.120
  607.3 1.8 copy.121
  (197 shorter events, 66.1 us)
Async XLA Ops:
  7.2 202.2 %copy-start = (bf16[1,128,4096]{2,1,0:T(8,128)(2,1)S(1)}, bf16[1,128,4096]{2,1,0:T(8,128)(2,1)}, u32[]{:S(2)}) copy-start(bf16[1,128,4096]{2,1,0:T(8,128)(2,1)} %param.17) | copy-start | bytes 3145732
  13.7 55.5 %all-to-all-start = ((bf16[1,128,16,512]{1,3,0,2:T(8,128)(2,1)}), bf16[1,128,16,512]{1,3,0,2:T(8,128)(2,1)S(1)}, u32[]{:S(2)}, u32[]{:S(2)}) async-start(bf16[1,128,16,512]{1,3,0,2:T(8,128)(2,1)} %maximum_bitcast_fusion.1), calls=%async_computation | async-start | bytes 4194304 | tf_op jit(solution)/shard_map/all_to_all | solution.py:109
  21.0 264.5 %reduce-scatter.2.cloned.1.call-start = ((), (), s32[]{:S(2)}) async-start(), calls=%async_computation.4 | async-start | bytes 10485760 | tf_op jit(solution)/shard_map/reduce_scatter | solution.py:153
  71.8 3.1 copy-start.14
  71.8 3.1 copy-start.16
  76.7 3.3 copy-start.5
  87.3 2.6 copy-start.1
  87.3 2.6 copy-start.7
  87.3 4.8 copy-start.3
  99.6 2.8 copy-start.1
  99.6 2.8 copy-start.7
  99.6 5.0 copy-start.3
  110.1 2.5 copy-start.4
  110.5 4.5 copy-start.6
  112.8 3.0 copy-start.11
  112.8 3.0 copy-start.13
  116.9 2.2 copy-start.15
  120.9 3.3 copy-start.5
  131.4 2.6 copy-start.1
  131.4 2.6 copy-start.7
  131.4 4.8 copy-start.3
  143.7 2.8 copy-start.1
  143.8 2.8 copy-start.7
  143.8 5.0 copy-start.3
  154.3 2.5 copy-start.4
  154.6 4.5 copy-start.6
  157.0 3.0 copy-start.11
  157.0 3.0 copy-start.13
  161.0 2.2 copy-start.15
  161.0 2.2 copy-start.17
  215.0 130.9 %all-gather.4.cloned.1.call-start = ((), (), s32[]{:S(2)}) async-start(), calls=%async_computation.3 | async-start | bytes 10485760 | tf_op jit(solution)/shard_map/all_gather | solution.py:150
  219.1 356.3 %all-gather.6.cloned.1.call-start = ((), (), s32[]{:S(2)}) async-start(), calls=%async_computation.5 | async-start | bytes 18874368 | tf_op jit(solution)/shard_map/all_gather | solution.py:156
  (16 other events, 19.0 us)
Sparse Core Ops, SparseCore 0:
  215.1 70.3 reduce-scatter.1
  287.6 58.2 all-gather.3
  348.1 227.2 all-gather.5
